TPU v7x, 32 devices: a whole 2x2x4 slice. The times are simulated.
32 devices in a mesh: grp: 2 (over y), fs: 4 (over z), tp: 4 (over x, core).
Axes of the slice: x: 2, y: 2, z: 4, core: 2. Of those that a mesh axis runs over, the one named last changes fastest.
Arguments:
- tokens: bfloat16 [1536, 2048], P(('grp', 'tp')), parts along dimension 0, may hold values from -6 to 6
- routes: int32 [1536, 2], P(('grp', 'tp')), parts along dimension 0, may hold values from 0 to 3, all different within a row; in each aligned block of 192 rows (0 to 191, 192 to 383, ...) at most 128 rows name the same one
- route_weight: float32 [1536, 2], P(('grp', 'tp')), parts along dimension 0, may hold values from 0.2 to 1
- norm_gain: float32 [2048], P('fs'), may hold values from 0.1 to 1.9
- gate_train: float32 [4, 2048, 5632], P('tp', 'fs'), may hold values from -0.125 to 0.125
- up_train: float32 [4, 2048, 5632], P('tp', 'fs'), may hold values from -0.125 to 0.125
- down_train: float32 [4, 5632, 2048], P('tp', None, 'fs'), may hold values from -0.109375 to 0.109375
Outputs:
- gate_serve: bfloat16 [8, 2048, 5632], P(('grp', 'tp'), None, 'fs'), parts along dimension 0
- up_serve: bfloat16 [8, 2048, 5632], P(('grp', 'tp'), None, 'fs'), parts along dimension 0
- down_serve: bfloat16 [8, 5632, 2048], P(('grp', 'tp'), 'fs'), parts along dimension 0
- mixed: bfloat16 [1536, 2048], P(('grp', 'tp'), 'fs'), parts along dimension 0
There are 2 independent parts, one for each index of `grp`. A program takes and returns all parts, laid end to end along the dimension named above; an argument that names none is the same for every part. Nothing has to cross between parts.
Inputs may be any that keep to these rules, and one draw needn't show every extreme that they name: `routes`: each row names 2 different experts. In each aligned block of 192 rows no expert is named by more than 128 rows, a bound that some block reaches.
All inputs are finite; a program needn't handle non-finite values.
Results may differ from a plain program's by a relative error of at most 0.0087.
Values may be sent and summed in bfloat16 or wider, within the bound.
A program may use at most 128 MiB of HBM per device.

v0:
```python
import jax
import jax.numpy as jnp
from jax import lax
from jax.sharding import PartitionSpec as P

EXPERTS = 4
CAP = 128


def shards(tokens, routes, route_weight, norm_gain, gate_train, up_train, down_train):
    fs_count = lax.axis_size("fs")
    pieces = min(fs_count, 32)
    copies = fs_count // pieces
    gain_column = norm_gain[:, None]
    gate_low = (gate_train[0] * gain_column).astype(jnp.bfloat16)
    up_low = (up_train[0] * gain_column).astype(jnp.bfloat16)
    down_low = down_train[0].astype(jnp.bfloat16)
    gate_wide = jnp.tile(gate_low, (1, copies))
    up_wide = jnp.tile(up_low, (1, copies))
    down_wide = jnp.tile(down_low, (copies, 1))
    gate_new, up_new = (
        lax.all_to_all(gate_wide, "fs", split_axis=1, concat_axis=0, tiled=True),
        lax.all_to_all(up_wide, "fs", split_axis=1, concat_axis=0, tiled=True),
    )
    down_new = lax.all_to_all(down_wide, "fs", split_axis=0, concat_axis=1, tiled=True)
    tok_float = tokens.astype(jnp.float32)
    normed = (
        tok_float * lax.rsqrt(jnp.mean(tok_float * tok_float, axis=-1, keepdims=True) + 1e-06)
    ).astype(jnp.bfloat16)
    chosen = routes.reshape(-1)
    chosen_hot = (chosen[:, None] == jnp.arange(EXPERTS, dtype=jnp.int32)[None, :]).astype(
        jnp.int32
    )
    before = jnp.cumsum(chosen_hot, axis=0) - chosen_hot
    slot_rank = jnp.sum(before * chosen_hot, axis=1)
    slot_index = (chosen * CAP + slot_rank).reshape(routes.shape)
    slot_range = jnp.arange(EXPERTS * CAP, dtype=jnp.int32)
    select_rows = jnp.any(slot_range[:, None, None] == slot_index[None, :, :], axis=-1).astype(
        jnp.bfloat16
    )
    outgoing = jnp.dot(select_rows, normed, preferred_element_type=jnp.float32).astype(jnp.bfloat16)
    outgoing = outgoing.reshape(EXPERTS, CAP, normed.shape[1])
    arrived = lax.all_to_all(outgoing, "tp", split_axis=0, concat_axis=0, tiled=True).reshape(
        EXPERTS * CAP, normed.shape[1]
    )
    slot_count = EXPERTS * CAP // copies
    copy_index = lax.axis_index("fs") // pieces
    my_rows = lax.dynamic_slice_in_dim(arrived, copy_index * slot_count, slot_count, 0)
    gated = jnp.dot(my_rows, gate_new, preferred_element_type=jnp.float32)
    lifted = jnp.dot(my_rows, up_new, preferred_element_type=jnp.float32)
    hidden = (jax.nn.silu(gated) * lifted).astype(jnp.bfloat16)
    partial_out = jnp.dot(hidden, down_new, preferred_element_type=jnp.float32)
    placed = jnp.zeros((EXPERTS * CAP, partial_out.shape[1]), jnp.float32)
    placed = lax.dynamic_update_slice_in_dim(placed, partial_out, copy_index * slot_count, 0)
    expert_out = lax.psum_scatter(placed, "fs", scatter_dimension=1, tiled=True).astype(
        jnp.bfloat16
    )
    returned = lax.all_to_all(
        expert_out.reshape(EXPERTS, CAP, expert_out.shape[1]),
        "tp",
        split_axis=0,
        concat_axis=0,
        tiled=True,
    )
    returned = returned.reshape(EXPERTS * CAP, expert_out.shape[1]).astype(jnp.float32)
    blend_weight = jnp.sum(
        jnp.where(
            slot_range[None, None, :] == slot_index[:, :, None], route_weight[:, :, None], 0.0
        ),
        axis=1,
    )
    mixed = jnp.dot(
        blend_weight, returned, precision=lax.Precision.HIGHEST, preferred_element_type=jnp.float32
    )
    return (gate_new[None], up_new[None], down_new[None], mixed.astype(jnp.bfloat16))


def solution(mesh):
    in_specs = (
        P(("grp", "tp"), None),
        P(("grp", "tp"), None),
        P(("grp", "tp"), None),
        P("fs"),
        P("tp", "fs", None),
        P("tp", "fs", None),
        P("tp", None, "fs"),
    )
    out_specs = (
        P(("grp", "tp"), None, "fs"),
        P(("grp", "tp"), None, "fs"),
        P(("grp", "tp"), "fs", None),
        P(("grp", "tp"), "fs"),
    )
    return jax.shard_map(shards, mesh=mesh, in_specs=in_specs, out_specs=out_specs, check_vma=False)
```

profile of v0, /device:TPU:0, one launch (start us, length us, event | category | flops | bytes accessed | tf_op | source)
XLA Modules:
  0.0 587.4 jit_solution(4837379173826643466)
XLA Ops:
  7.2 0.8 copy.54
  8.0 0.1 eq.56
  8.1 0.1 eq.52
  8.3 1.2 reduce-window.6
  9.5 0.2 slice_reduce_fusion
  9.7 0.2 reduce-window.9
  9.9 0.1 add_bitcast_fusion
  10.0 0.1 reduce_sum.30
  10.1 0.1 copy.56
  10.2 0.7 multiply_add_fusion
  10.9 0.1 fusion.7
  11.1 1.4 fusion.3
  12.4 3.3 convolution_convert_fusion
  15.7 4.2 all-to-all-start.3
  19.9 14.5 %squeeze.7 = f32[512,4,1408]{2,1,0:T(4,128)} reshape(f32[1,512,5632]{2,1,0:T(8,128)} %param.11) | data formatting | bytes 23068672 | tf_op jit(solution)/shard_map/squeeze | solution.py:15
  34.5 0.0 copy-start
  34.5 14.5 %squeeze.8 = f32[512,4,1408]{2,1,0:T(4,128)} reshape(f32[1,512,5632]{2,1,0:T(8,128)} %param.12) | data formatting | bytes 23068672 | tf_op jit(solution)/shard_map/squeeze | solution.py:16
  49.0 0.0 copy-done
  49.0 16.8 %fusion = (bf16[512,4,1408]{2,0,1:T(8,128)(2,1)}, bf16[512,4,1408]{2,0,1:T(8,128)(2,1)}) fusion(f32[512,4,1408]{2,1,0:T(4,128)} %squeeze.8, f32[512]{0:T(512)S(1)} %copy-done, f32[512,4,1408]{2,1,0:T(4,128)} %squeeze.7), kind=kLoop, calls=%fused_computation.1 | loop fusion | flops 11534336 | bytes 34605056 | tf_op jit(solution)/shard_map/convert_element_type | solution.py:16
  65.8 0.0 all-to-all-done.3
  65.9 5.7 all-to-all-start
  71.6 7.5 %convert_element_type.44 = bf16[1,5632,512]{2,1,0:T(8,128)(2,1)} convert(f32[1,5632,512]{2,1,0:T(8,128)} %param.13) | non-fusion elementwise | flops 2883584 | bytes 17301504 | tf_op jit(solution)/shard_map/convert_element_type | solution.py:17
  79.1 120.5 %all-to-all-done = bf16[512,4,1408]{2,0,1:T(8,128)(2,1)} async-done(((bf16[512,4,1408]{2,0,1:T(8,128)(2,1)}), bf16[512,4,1408]{2,0,1:T(8,128)(2,1)}, u32[]{:S(2)}, u32[]{:S(2)}) %all-to-all-start) | async-done | bytes 5767200 | tf_op jit(solution)/shard_map/all_to_all | solution.py:22
  199.6 133.5 %all_to_all.58 = bf16[4,1408,512]{2,1,0:T(8,128)(2,1)} all-to-all(bf16[4,1408,512]{2,1,0:T(8,128)(2,1)} %bitcast.49), channel_id=1, replica_groups=mesh['grp'=2,'fs'=4,'tp'=4] {'fs'}, dimensions={0} | all-to-all | bytes 11534336 | tf_op jit(solution)/shard_map/all_to_all | solution.py:25
  333.2 5.2 all-to-all-start.1
  338.3 0.2 reduce-scatter.2.cloned.1.call-start
  338.6 8.3 %copy.53 = bf16[4,1408,512]{1,2,0:T(8,128)(2,1)} copy(bf16[4,1408,512]{2,1,0:T(8,128)(2,1)} %all_to_all.58) | data formatting | bytes 11534336 | tf_op jit(solution)/shard_map/all_to_all | solution.py:25
  346.9 7.6 %fusion.14 = f32[512,1408]{1,0:T(8,128)} fusion(bf16[512,2048]{1,0:T(8,128)(2,1)S(1)} %bitcast.50, bf16[2048,1408]{1,0:T(8,128)(2,1)} %bitcast.10), kind=kOutput, calls=%fused_computation.30 | convolution fusion | flops 2952790016 | bytes 10747904 | tf_op jit(solution)/shard_map/dot_general | solution.py:49
  354.5 110.3 %all-to-all-done.1 = bf16[512,4,1408]{2,0,1:T(8,128)(2,1)} async-done(((bf16[512,4,1408]{2,0,1:T(8,128)(2,1)}), bf16[512,4,1408]{2,0,1:T(8,128)(2,1)}, u32[]{:S(2)}, u32[]{:S(2)}) %all-to-all-start.1) | async-done | bytes 5767200 | tf_op jit(solution)/shard_map/all_to_all | solution.py:23
  464.8 13.9 %fusion.8 = f32[512,2048]{1,0:T(8,128)} fusion(bf16[1408,2048]{0,1:T(8,128)(2,1)} %bitcast.47, bf16[512,2048]{1,0:T(8,128)(2,1)S(1)} %bitcast.51, bf16[2048,1408]{1,0:T(8,128)(2,1)} %bitcast.11, f32[512,1408]{1,0:T(8,128)} %fusion.14), kind=kOutput, calls=%fused_computation.17 | convolution fusion | flops 5909905408 | bytes 20709376 | tf_op jit(solution)/shard_map/dot_general | solution.py:52
  478.7 0.0 copy-start.1
  478.7 0.0 reduce-scatter.2.cloned.1.call-update
  478.7 75.2 %reduce-scatter.2.cloned.1.call-done = f32[512,512]{1,0:T(8,128)} async-done(((f32[512,2048]{1,0:T(8,128)}), f32[512,512]{1,0:T(8,128)}) %reduce-scatter.2.cloned.1.call-update) | async-done | bytes 1048592 | tf_op jit(solution)/shard_map/reduce_scatter | solution.py:55
  553.9 2.1 convert_element_type.52
  555.9 3.5 all-to-all-start.4
  559.4 0.0 copy-done.1
  559.4 0.2 select_reduce_fusion
  559.6 8.2 %copy.57 = bf16[1,1408,2048]{2,1,0:T(8,128)(2,1)} copy(bf16[1,1408,2048]{1,2,0:T(8,128)(2,1)} %bitcast.48) | data formatting | bytes 11534336
  567.9 0.3 all-to-all-done.4
  568.2 1.2 convolution_convert_fusion.1
  569.4 5.6 copy.68
  575.0 5.6 copy.69
  (3 shorter events, 0.0 us)
Async XLA Ops:
  15.7 50.1 %all-to-all-start.3 = ((bf16[4,128,2048]{2,1,0:T(8,128)(2,1)}), bf16[4,128,2048]{2,1,0:T(8,128)(2,1)S(1)}, u32[]{:S(2)}, u32[]{:S(2)}) async-start(bf16[4,128,2048]{2,1,0:T(8,128)(2,1)} %bitcast.8), calls=%async_computation.3 | async-start | bytes 4194304 | tf_op jit(solution)/shard_map/all_to_all | solution.py:43
  34.5 14.5 %copy-start = (f32[512]{0:T(512)S(1)}, f32[512]{0:T(512)}, u32[]{:S(2)}) copy-start(f32[512]{0:T(512)} %param.10) | copy-start | bytes 6148
  65.9 133.8 %all-to-all-start = ((bf16[512,4,1408]{2,0,1:T(8,128)(2,1)}), bf16[512,4,1408]{2,0,1:T(8,128)(2,1)}, u32[]{:S(2)}, u32[]{:S(2)}) async-start(bf16[512,4,1408]{2,0,1:T(8,128)(2,1)} %get-tuple-element.17), calls=%async_computation | async-start | bytes 11534336 | tf_op jit(solution)/shard_map/all_to_all | solution.py:22
  333.2 131.6 %all-to-all-start.1 = ((bf16[512,4,1408]{2,0,1:T(8,128)(2,1)}), bf16[512,4,1408]{2,0,1:T(8,128)(2,1)}, u32[]{:S(2)}, u32[]{:S(2)}) async-start(bf16[512,4,1408]{2,0,1:T(8,128)(2,1)} %get-tuple-element.16), calls=%async_computation.1 | async-start | bytes 11534336 | tf_op jit(solution)/shard_map/all_to_all | solution.py:23
  338.3 215.5 %reduce-scatter.2.cloned.1.call-start = ((), (), s32[]{:S(2)}) async-start(), calls=%async_computation.6 | async-start | bytes 5242880 | tf_op jit(solution)/shard_map/reduce_scatter | solution.py:55
  478.7 80.8 %copy-start.1 = (f32[192,2]{0,1:T(2,128)S(1)}, f32[192,2]{0,1:T(2,128)}, u32[]{:S(2)}) copy-start(f32[192,2]{0,1:T(2,128)} %param.9) | copy-start | bytes 4612
  555.9 12.3 %all-to-all-start.4 = ((bf16[4,128,512]{2,1,0:T(8,128)(2,1)}), bf16[4,128,512]{2,1,0:T(8,128)(2,1)S(1)}, u32[]{:S(2)}, u32[]{:S(2)}) async-start(bf16[4,128,512]{2,1,0:T(8,128)(2,1)} %bitcast.13), calls=%async_computation.5 | async-start | bytes 1048576 | tf_op jit(solution)/shard_map/all_to_all | solution.py:58
Sparse Core Ops, SparseCore 0:
  478.8 74.9 reduce-scatter.1
where the time goes:
time: 589 us; the launch traced here: 587 us
  waiting for transfers between devices  306 us (52%)
  blocking collectives  134 us (23%)
  local copies, waits for them, and re-layouts  58.3 us (10%)
  other arithmetic  30.4 us (5%)
  matrix products  25.9 us (4%)
  starting transfers between devices  18.8 us (3%)
  between operations  14.1 us (2%)
    all_to_all x1, blocking collectives, shards(): lax.all_to_all(down_wide, 'fs', split_axis=0, concat_axis=1, tiled=True)  134 us
    all_to_all x1, waiting for transfers between devices, shards(): lax.all_to_all(gate_wide, 'fs', split_axis=1, concat_axis=0, tiled=True)  120 us
    all_to_all x1, waiting for transfers between devices, shards(): lax.all_to_all(up_wide, 'fs', split_axis=1, concat_axis=0, tiled=True)  110 us
    reduce_scatter x1, waiting for transfers between devices, shards(): lax.psum_scatter(placed, 'fs', scatter_dimension=1, tiled=True)  75.2 us
    unnamed x8, local copies, waits for them, and re-layouts  20.2 us
    convert_element_type x1, other arithmetic, shards(): up_low = (up_train[0] * gain_column).astype(jnp.bfloat16)  16.8 us
    squeeze x1, local copies, waits for them, and re-layouts, shards(): gate_low = (gate_train[0] * gain_column).astype(jnp.bfloat16)  14.5 us
    squeeze x1, local copies, waits for them, and re-layouts, shards(): up_low = (up_train[0] * gain_column).astype(jnp.bfloat16)  14.5 us
  transfers between devices with their start and end apart: 5, of which 4 were waited for; matrix products, arithmetic and copies ran while one was open for 13% of the time, Pallas kernels for 0%

commit v1 on v0

--- a/solution.py
+++ b/solution.py
@@ -20,7 +20,10 @@
     down_wide = jnp.tile(down_low, (copies, 1))
     gate_new, up_new = (
         lax.all_to_all(gate_wide, "fs", split_axis=1, concat_axis=0, tiled=True),
-        lax.all_to_all(up_wide, "fs", split_axis=1, concat_axis=0, tiled=True),
+        jnp.concatenate(
+            lax.all_to_all(jnp.stack(jnp.split(up_wide, lax.axis_size("fs"), axis=1)), "fs", 0, 0),
+            axis=0,
+        ),
     )
     down_new = lax.all_to_all(down_wide, "fs", split_axis=0, concat_axis=1, tiled=True)
     tok_float = tokens.astype(jnp.float32)

time: 589 us -> 566 us (0.961)
  blocking collectives: 134 us -> 0 us
  waiting for transfers between devices: 306 us -> 426 us
  local copies, waits for them, and re-layouts: 58.3 us -> 44.2 us
    all_to_all x1 -> x0, blocking collectives: 134 us -> none  [shards(): lax.all_to_all(down_wide, 'fs', split_axis=0, concat_axis=1, tiled=True)]
    all_to_all x1 -> x2, waiting for transfers between devices: 110 us -> 227 us  [the longest x1 117 us: shards(): lax.all_to_all(down_wide, 'fs', split_axis=0, concat_axis=1, tiled=True)]
    squeeze x1 -> x0, local copies, waits for them, and re-layouts: 14.5 us -> none  [shards(): up_low = (up_train[0] * gain_column).astype(jnp.bfloat16)]
    convert_element_type x1, other arithmetic: 16.8 us -> 5.8 us  [shards(): up_low = (up_train[0] * gain_column).astype(jnp.bfloat16)]
    convert_element_type x0 -> x1, other arithmetic: none -> 8.06 us  [shards(): gate_low = (gate_train[0] * gain_column).astype(jnp.bfloat16)]
  transfers between devices with their start and end apart: 5 -> 6, of which waited for: 4 -> 6; matrix products, arithmetic and copies ran while one was open for 13% -> 11% of each run, Pallas kernels for 0% -> 0%
where the time goes in v1:
time: 566 us; the launch traced here: 564 us
  waiting for transfers between devices  426 us (75%)
  local copies, waits for them, and re-layouts  44.2 us (8%)
  other arithmetic  30.6 us (5%)
  matrix products  25.9 us (5%)
  starting transfers between devices  23.9 us (4%)
  between operations  14.1 us (2%)
    all_to_all x1, waiting for transfers between devices, shards(): lax.all_to_all(gate_wide, 'fs', split_axis=1, concat_axis=0, tiled=True)  120 us
    all_to_all x1, waiting for transfers between devices, shards(): lax.all_to_all(down_wide, 'fs', split_axis=0, concat_axis=1, tiled=True)  117 us
    all_to_all x1, waiting for transfers between devices, shards(): lax.all_to_all(jnp.stack(jnp.split(up_wide, lax.axis_size('fs'), axis=1))...  110 us
    reduce_scatter x1, waiting for transfers between devices, shards(): lax.psum_scatter(placed, 'fs', scatter_dimension=1, tiled=True)  75.4 us
    unnamed x8, local copies, waits for them, and re-layouts  20.2 us
    squeeze x1, local copies, waits for them, and re-layouts, shards(): gate_low = (gate_train[0] * gain_column).astype(jnp.bfloat16)  14.5 us
    dot_general x1, matrix products, shards(): partial_out = jnp.dot(hidden, down_new, preferred_element_type=jnp.float32)  13.9 us
  transfers between devices with their start and end apart: 6, of which 6 were waited for; matrix products, arithmetic and copies ran while one was open for 11% of the time, Pallas kernels for 0%

profile of v1, /device:TPU:0, one launch (start us, length us, event | category | flops | bytes accessed | tf_op | source)
XLA Modules:
  0.0 564.4 jit_solution(9464458475550337377)
XLA Ops:
  7.2 0.8 copy.48
  8.0 0.1 eq.56
  8.1 0.1 eq.52
  8.3 1.2 reduce-window.6
  9.5 0.2 slice_reduce_fusion
  9.7 0.2 reduce-window.9
  9.9 0.1 add_bitcast_fusion
  10.0 0.1 reduce_sum.30
  10.1 0.1 copy.50
  10.2 0.7 multiply_add_fusion
  10.9 0.1 fusion.7
  11.1 1.4 fusion.3
  12.4 3.3 convolution_convert_fusion
  15.7 4.2 all-to-all-start.3
  19.9 0.0 copy-start
  20.0 14.5 %squeeze.7 = f32[512,4,1408]{2,1,0:T(4,128)} reshape(f32[1,512,5632]{2,1,0:T(8,128)} %param.11) | data formatting | bytes 23068672 | tf_op jit(solution)/shard_map/squeeze | solution.py:15
  34.5 0.0 copy-done
  34.5 8.1 %fusion.1 = bf16[512,4,1408]{2,0,1:T(8,128)(2,1)} fusion(f32[512,4,1408]{2,1,0:T(4,128)} %squeeze.7, f32[512]{0:T(512)S(1)} %copy-done), kind=kLoop, calls=%fused_computation.3 | loop fusion | flops 5767168 | bytes 17303552 | tf_op jit(solution)/shard_map/convert_element_type | solution.py:15
  42.5 3.1 all-to-all-done.3
  45.6 5.7 %all-to-all-start = ((bf16[512,4,1408]{2,0,1:T(8,128)(2,1)}), bf16[512,4,1408]{2,0,1:T(8,128)(2,1)}, u32[]{:S(2)}, u32[]{:S(2)}) async-start(bf16[512,4,1408]{2,0,1:T(8,128)(2,1)} %fusion.1), calls=%async_computation | async-start | bytes 11534336 | tf_op jit(solution)/shard_map/all_to_all | solution.py:22
  51.3 7.5 %convert_element_type.43 = bf16[1,5632,512]{2,1,0:T(8,128)(2,1)} convert(f32[1,5632,512]{2,1,0:T(8,128)} %param.13) | non-fusion elementwise | flops 2883584 | bytes 17301504 | tf_op jit(solution)/shard_map/convert_element_type | solution.py:17
  58.9 119.6 %all-to-all-done = bf16[512,4,1408]{2,0,1:T(8,128)(2,1)} async-done(((bf16[512,4,1408]{2,0,1:T(8,128)(2,1)}), bf16[512,4,1408]{2,0,1:T(8,128)(2,1)}, u32[]{:S(2)}, u32[]{:S(2)}) %all-to-all-start) | async-done | bytes 5767200 | tf_op jit(solution)/shard_map/all_to_all | solution.py:22
  178.4 5.2 all-to-all-start.2
  183.6 5.8 %fusion = bf16[512,5632]{1,0:T(8,128)(2,1)S(1)} fusion(f32[1,512,5632]{2,1,0:T(8,128)} %param.12, f32[512]{0:T(512)S(1)} %copy-done), kind=kLoop, calls=%fused_computation.1 | loop fusion | flops 5767168 | bytes 17303552 | tf_op jit(solution)/shard_map/convert_element_type | solution.py:16
  189.4 0.4 slice_bitcast_fusion.3
  189.9 3.2 pad_maximum_fusion
  193.1 116.8 %all-to-all-done.2 = bf16[4,1408,512]{2,1,0:T(8,128)(2,1)} async-done(((bf16[4,1408,512]{2,1,0:T(8,128)(2,1)}), bf16[4,1408,512]{2,1,0:T(8,128)(2,1)}, u32[]{:S(2)}, u32[]{:S(2)}) %all-to-all-start.2) | async-done | bytes 5767200 | tf_op jit(solution)/shard_map/all_to_all | solution.py:28
  309.9 5.2 all-to-all-start.1
  315.1 0.2 reduce-scatter.2.cloned.1.call-start
  315.3 8.3 %copy.47 = bf16[4,1408,512]{1,2,0:T(8,128)(2,1)} copy(bf16[4,1408,512]{2,1,0:T(8,128)(2,1)} %all-to-all-done.2) | data formatting | bytes 11534336 | tf_op jit(solution)/shard_map/all_to_all | solution.py:28
  323.7 7.6 %fusion.14 = f32[512,1408]{1,0:T(8,128)} fusion(bf16[512,2048]{1,0:T(8,128)(2,1)S(1)} %bitcast.59, bf16[2048,1408]{1,0:T(8,128)(2,1)} %bitcast.14), kind=kOutput, calls=%fused_computation.35 | convolution fusion | flops 2952790016 | bytes 10747904 | tf_op jit(solution)/shard_map/dot_general | solution.py:52
  331.3 110.3 %all-to-all-done.1 = bf16[4,512,1408]{2,1,0:T(8,128)(2,1)} async-done(((bf16[4,512,1408]{2,1,0:T(8,128)(2,1)}), bf16[4,512,1408]{2,1,0:T(8,128)(2,1)}, u32[]{:S(2)}, u32[]{:S(2)}) %all-to-all-start.1) | async-done | bytes 5767200 | tf_op jit(solution)/shard_map/all_to_all | solution.py:24
  441.6 13.9 %fusion.8 = f32[512,2048]{1,0:T(8,128)} fusion(bf16[1408,2048]{0,1:T(8,128)(2,1)} %bitcast.56, bf16[512,2048]{1,0:T(8,128)(2,1)S(1)} %bitcast.60, bf16[2048,1408]{1,0:T(8,128)(2,1)} %bitcast.15, f32[512,1408]{1,0:T(8,128)} %fusion.14), kind=kOutput, calls=%fused_computation.22 | convolution fusion | flops 5909905408 | bytes 20709376 | tf_op jit(solution)/shard_map/dot_general | solution.py:55
  455.4 0.0 copy-start.1
  455.5 0.0 reduce-scatter.2.cloned.1.call-update
  455.5 75.4 %reduce-scatter.2.cloned.1.call-done = f32[512,512]{1,0:T(8,128)} async-done(((f32[512,2048]{1,0:T(8,128)}), f32[512,512]{1,0:T(8,128)}) %reduce-scatter.2.cloned.1.call-update) | async-done | bytes 1048592 | tf_op jit(solution)/shard_map/reduce_scatter | solution.py:58
  530.9 2.1 convert_element_type.51
  533.0 3.5 all-to-all-start.4
  536.5 0.0 copy-done.1
  536.5 0.2 select_reduce_fusion
  536.7 8.2 %copy.51 = bf16[1,1408,2048]{2,1,0:T(8,128)(2,1)} copy(bf16[1,1408,2048]{1,2,0:T(8,128)(2,1)} %bitcast.57) | data formatting | bytes 11534336
  544.9 0.3 all-to-all-done.4
  545.3 1.2 convolution_convert_fusion.1
  546.4 5.6 copy.59
  552.0 5.6 copy.60
  (3 shorter events, 0.0 us)
Async XLA Ops:
  15.7 29.9 %all-to-all-start.3 = ((bf16[4,128,2048]{2,1,0:T(8,128)(2,1)}), bf16[4,128,2048]{2,1,0:T(8,128)(2,1)S(1)}, u32[]{:S(2)}, u32[]{:S(2)}) async-start(bf16[4,128,2048]{2,1,0:T(8,128)(2,1)} %bitcast.12), calls=%async_computation.3 | async-start | bytes 4194304 | tf_op jit(solution)/shard_map/all_to_all | solution.py:46
  19.9 14.5 %copy-start = (f32[512]{0:T(512)S(1)}, f32[512]{0:T(512)}, u32[]{:S(2)}) copy-start(f32[512]{0:T(512)} %param.10) | copy-start | bytes 6148
  45.6 132.8 %all-to-all-start = ((bf16[512,4,1408]{2,0,1:T(8,128)(2,1)}), bf16[512,4,1408]{2,0,1:T(8,128)(2,1)}, u32[]{:S(2)}, u32[]{:S(2)}) async-start(bf16[512,4,1408]{2,0,1:T(8,128)(2,1)} %fusion.1), calls=%async_computation | async-start | bytes 11534336 | tf_op jit(solution)/shard_map/all_to_all | solution.py:22
  178.4 131.5 %all-to-all-start.2 = ((bf16[4,1408,512]{2,1,0:T(8,128)(2,1)}), bf16[4,1408,512]{2,1,0:T(8,128)(2,1)}, u32[]{:S(2)}, u32[]{:S(2)}) async-start(bf16[4,1408,512]{2,1,0:T(8,128)(2,1)} %bitcast.58), calls=%async_computation.2 | async-start | bytes 11534336 | tf_op jit(solution)/shard_map/all_to_all | solution.py:28
  309.9 131.6 %all-to-all-start.1 = ((bf16[4,512,1408]{2,1,0:T(8,128)(2,1)}), bf16[4,512,1408]{2,1,0:T(8,128)(2,1)}, u32[]{:S(2)}, u32[]{:S(2)}) async-start(bf16[4,512,1408]{2,1,0:T(8,128)(2,1)} %pad_maximum_fusion), calls=%async_computation.1 | async-start | bytes 11534336 | tf_op jit(solution)/shard_map/all_to_all | solution.py:24
  315.1 215.8 %reduce-scatter.2.cloned.1.call-start = ((), (), s32[]{:S(2)}) async-start(), calls=%async_computation.6 | async-start | bytes 5242880 | tf_op jit(solution)/shard_map/reduce_scatter | solution.py:58
  455.4 81.0 %copy-start.1 = (f32[192,2]{0,1:T(2,128)S(1)}, f32[192,2]{0,1:T(2,128)}, u32[]{:S(2)}) copy-start(f32[192,2]{0,1:T(2,128)} %param.9) | copy-start | bytes 4612
  533.0 12.3 %all-to-all-start.4 = ((bf16[4,128,512]{2,1,0:T(8,128)(2,1)}), bf16[4,128,512]{2,1,0:T(8,128)(2,1)S(1)}, u32[]{:S(2)}, u32[]{:S(2)}) async-start(bf16[4,128,512]{2,1,0:T(8,128)(2,1)} %bitcast.17), calls=%async_computation.5 | async-start | bytes 1048576 | tf_op jit(solution)/shard_map/all_to_all | solution.py:61
Sparse Core Ops, SparseCore 0:
  455.6 75.2 reduce-scatter.1
